TPU v7x, 32 devices: a whole 2x2x4 slice. The times are simulated.
32 devices in a mesh: ep: 4 (over y, x), tp: 8 (over z, core).
Axes of the slice: x: 2, y: 2, z: 4, core: 2. Of those that a mesh axis runs over, the one named last changes fastest.
Arguments:
- tokens: bfloat16 [256, 2048], P('ep'), may hold values from -7 to 7
- state: float32 [256, 32, 64, 64], P('ep', 'tp'), may hold values from -6 to 6
- routes: int32 [256, 2], P('ep'), may hold values from 0 to 3, all different within a row; in each aligned block of 64 rows (0 to 63, 64 to 127, ...) at most 48 rows name the same one
- route_logits: float32 [256, 2], P('ep'), may hold values from -4 to 4
- mix_gain: float32 [2048], replicated, may hold values from 0.1 to 1.9
- w_recept: bfloat16 [2048, 2048], P(None, 'tp')
- w_key: bfloat16 [2048, 2048], P(None, 'tp'), may hold values from -0.125 to 0.125
- w_value: bfloat16 [2048, 2048], P(None, 'tp'), may hold values from -0.125 to 0.125
- w_decay: bfloat16 [2048, 2048], P(None, 'tp'), may hold values from -0.125 to 0.125
- w_rate: bfloat16 [2048, 2048], P(None, 'tp'), may hold values from -0.125 to 0.125
- decay_base: float32 [2048], P('tp'), may hold values from -3 to 1
- rate_base: float32 [2048], P('tp'), may hold values from -3 to 3
- key_gain: float32 [2048], P('tp'), may hold values from 0.1 to 1.9
- group_gain: float32 [2048], P('tp'), may hold values from 0.1 to 1.9
- w_output: bfloat16 [2048, 2048], P('tp'), may hold values from -0.125 to 0.125
- ffn_gain: float32 [2048], replicated, may hold values from 0.1 to 1.9
- w_gate: bfloat16 [4, 2048, 7168], P('ep', None, 'tp'), may hold values from -0.125 to 0.125
- w_up: bfloat16 [4, 2048, 7168], P('ep', None, 'tp'), may hold values from -0.125 to 0.125
- w_down: bfloat16 [4, 7168, 2048], P('ep', 'tp'), may hold values from -0.0625 to 0.0625
Outputs:
- output: bfloat16 [256, 2048], P('ep', 'tp')
- new_state: float32 [256, 32, 64, 64], P('ep', 'tp')
Inputs may be any that keep to these rules, and one draw needn't show every extreme that they name: `routes`: for each expert, the 64 tokens of one device group's rows name it in at most 48 of their rows; the 2 experts of a row differ.
All inputs are finite; a program needn't handle non-finite values.
Results may differ from a plain program's by a relative error of at most 0.0091.
Values may be sent and summed in bfloat16 or wider, within the bound.
A program may use at most 64 MiB of HBM per device.

v0:
```python
import jax
import jax.numpy as jnp
from jax import lax
from jax.experimental import pallas as pl
from jax.experimental.pallas import tpu as pltpu
from jax.sharding import PartitionSpec as P

MESH = pl.DeviceIdType.MESH

RMS_EPS = 1e-06
GROUP_EPS = 0.00064
UNIT_EPS = 6.4e-05


def mix_kernel(
    tokens,
    gain,
    w_recept,
    w_key,
    w_value,
    w_decay,
    w_rate,
    decay_base,
    rate_base,
    key_gain,
    group_gain,
    state,
    mixed,
    new_state,
    recept_s,
    key_s,
    decay_s,
    unit_s,
    pull_s,
    value_t,
    read_t,
):
    step = pl.program_id(0)
    count, heads, wide, _ = state.shape
    rows = tokens.shape[0]
    cols = heads * wide
    f32, bf16 = jnp.float32, jnp.bfloat16

    @pl.when(step == 0)
    def _():
        values = tokens[...].astype(f32)
        scale = lax.rsqrt(jnp.mean(values * values, axis=1, keepdims=True) + RMS_EPS)
        normed = (values * scale * gain[...]).astype(bf16)

        def project(weight):
            return jnp.dot(normed, weight[...], preferred_element_type=f32).astype(bf16).astype(f32)

        def split(ref, whole):
            for h in range(heads):
                ref[h] = whole[:, h * wide : (h + 1) * wide]

        key = project(w_key)
        split(key_s, key)
        scaled = key * key_gain[...]
        squares = scaled * scaled
        rate = 1.0 / (1.0 + jnp.exp(-(project(w_rate) + rate_base[...])))
        for h in range(heads):
            lanes = slice(h * wide, (h + 1) * wide)
            length = jnp.sum(squares[:, lanes], axis=1, keepdims=True)
            unit = scaled[:, lanes] * lax.rsqrt(length + UNIT_EPS)
            unit_s[h] = unit
            pull_s[h] = unit * rate[:, lanes]
        split(recept_s, project(w_recept))
        open_part = 1.0 / (1.0 + jnp.exp(-(project(w_decay) + decay_base[...])))
        split(decay_s, jnp.exp(-jnp.exp(-0.5) * open_part))
        turned = project(w_value).T
        for b in range(rows // count):
            value_t[b] = turned[:, b * count : (b + 1) * count]

    first = step * count
    block = value_t[step]
    lane = lax.broadcasted_iota(jnp.int32, (wide, count), 1)
    for h in range(heads):
        read = jnp.zeros((wide, count), f32)
        for k in range(count):
            spot = pl.ds(first + k, 1)
            old = state[k, h]
            removed = jnp.sum(old * unit_s[h, spot, :], axis=1, keepdims=True)
            column = block[h * wide : (h + 1) * wide, k : k + 1]
            new = old * decay_s[h, spot, :] - removed * pull_s[h, spot, :] + column * key_s[h, spot, :]
            new_state[k, h] = new
            out = jnp.sum(new * recept_s[h, spot, :], axis=1, keepdims=True)
            read = jnp.where(lane == k, out, read)
        centred = read - jnp.mean(read, axis=0, keepdims=True)
        spread = jnp.mean(centred * centred, axis=0, keepdims=True)
        read_t[step, h * wide : (h + 1) * wide, :] = centred * lax.rsqrt(spread + GROUP_EPS)

    @pl.when(step == rows // count - 1)
    def _():
        whole = jnp.concatenate([read_t[b] for b in range(rows // count)], axis=1)
        mixed[...] = (whole.T * group_gain[...]).astype(bf16)


def mix_heads(tokens, state, mix_gain, projections, offsets):
    rows, width = tokens.shape
    _, heads, wide, _ = state.shape
    cols = heads * wide
    count = min(rows, 8)
    f32 = jnp.float32

    def whole(*shape):
        return pl.BlockSpec(shape, lambda i: (0,) * len(shape))

    states = pl.BlockSpec((count, heads, wide, wide), lambda i: (i, 0, 0, 0))
    per_head = pltpu.VMEM((heads, rows, wide), f32)
    return pl.pallas_call(
        mix_kernel,
        grid=(rows // count,),
        out_shape=(
            jax.ShapeDtypeStruct((rows, cols), jnp.bfloat16),
            jax.ShapeDtypeStruct(state.shape, f32),
        ),
        in_specs=[whole(rows, width), whole(1, width)]
        + [whole(width, cols)] * 5
        + [whole(1, cols)] * 4
        + [states],
        out_specs=(whole(rows, cols), states),
        scratch_shapes=[per_head] * 5
        + [pltpu.VMEM((rows // count, cols, count), f32)] * 2,
        compiler_params=pltpu.CompilerParams(
            dimension_semantics=("arbitrary",), vmem_limit_bytes=67043328
        ),
    )(tokens, mix_gain[None], *projections, *[x[None] for x in offsets], state)


def experts_kernel(
    mixed,
    tokens,
    routes,
    logits,
    gain,
    wo_hbm,
    wg_hbm,
    wu_hbm,
    wd_hbm,
    out,
    wo,
    wg,
    wu,
    wd,
    p1send,
    p1recv,
    z1send,
    z1recv,
    seg,
    wsend,
    wall,
    xn,
    hid,
    p4send,
    p4recv,
    e4send,
    e4recv,
    summed,
    kept,
    z4send,
    z4recv,
    load_sem,
    ws_sem,
    wr_sem,
    p1s_sem,
    p1r_sem,
    z1s_sem,
    z1r_sem,
    gz_sem,
    ge_sem,
    gp_sem,
    gr_sem,
    p4s_sem,
    p4r_sem,
    e4s_sem,
    e4r_sem,
    z4s_sem,
    z4r_sem,
):
    ep, tp = lax.axis_size("ep"), lax.axis_size("tp")
    nz = tp // 2
    e, t = lax.axis_index("ep"), lax.axis_index("tp")
    z, c = t // 2, lax.rem(t, 2)
    rows, width = tokens.shape
    cols = width // tp
    ff = wg.shape[1]
    f32, bf16 = jnp.float32, jnp.bfloat16
    loads = [
        pltpu.make_async_copy(a, b, load_sem.at[i])
        for i, (a, b) in enumerate(
            ((wo_hbm, wo), (wg_hbm.at[0], wg), (wu_hbm.at[0], wu), (wd_hbm.at[0], wd))
        )
    ]
    for load in loads:
        load.start()
    partner = (e, z * 2 + (1 - c))
    far = list(range(1, nz)) + [0]

    def zpeer(d):
        return lax.rem(z + d, nz)

    def epeer(d):
        return lax.rem(e + d, ep)

    def z_dev(d):
        return (e, zpeer(d) * 2 + c)

    def e_dev(d):
        return (epeer(d), t)

    def remote(src, dst, ssem, rsem, dev):
        return pltpu.make_async_remote_copy(
            src_ref=src, dst_ref=dst, send_sem=ssem, recv_sem=rsem, device_id=dev, device_id_type=MESH
        )

    barrier = pltpu.get_barrier_semaphore()
    peers = [partner] + [z_dev(d) for d in range(1, nz)] + [e_dev(d) for d in range(1, ep)]
    for peer in peers:
        pl.semaphore_signal(barrier, inc=1, device_id=peer, device_id_type=MESH)

    picked = jnp.exp(logits[...])
    picked = picked / jnp.sum(picked, axis=0, keepdims=True)
    names = routes[...]
    diagonal = lax.broadcasted_iota(jnp.int32, (rows, rows), 0) == lax.broadcasted_iota(
        jnp.int32, (rows, rows), 1
    )

    def weight_of(expert):
        line = jnp.sum(jnp.where(names == expert, picked, 0.0), axis=0, keepdims=True)
        column = jnp.sum(jnp.where(diagonal, line, 0.0), axis=1, keepdims=True)
        return jnp.broadcast_to(column, (rows, 128))

    wall[e] = weight_of(e)
    for d in range(1, ep):
        wsend[d] = weight_of(epeer(d))

    def block_of(ref, index):
        return ref[:, pl.ds(pl.multiple_of(index * cols, 128), cols)]

    loads[0].wait()
    pl.semaphore_wait(barrier, len(peers))
    started = []

    def start(copy):
        copy.start()
        started.append(copy)

    for d in far:
        zt = zpeer(d)
        part = jnp.dot(mixed[...], block_of(wo, zt * 2 + (1 - c)), preferred_element_type=f32)
        p1send[d] = part.astype(bf16)
        start(remote(p1send.at[d], p1recv.at[d], p1s_sem.at[d], p1r_sem.at[d], partner))
    for d in range(1, ep):
        start(remote(wsend.at[d], wall.at[e], ws_sem.at[d], wr_sem.at[d], e_dev(d)))
    for d in far:
        zt = zpeer(d)
        part = jnp.dot(mixed[...], block_of(wo, zt * 2 + c), preferred_element_type=f32)
        remote(p1send.at[d], p1recv.at[d], p1s_sem.at[d], p1r_sem.at[d], partner).wait_recv()
        part = part + p1recv[d].astype(f32)
        if d:
            z1send[d] = part.astype(bf16)
            start(remote(z1send.at[d], z1recv.at[d], z1s_sem.at[d], z1r_sem.at[d], z_dev(d)))
    part = part + block_of(tokens, t).astype(f32)
    for d in range(1, nz):
        remote(z1send.at[d], z1recv.at[d], z1s_sem.at[d], z1r_sem.at[d], z_dev(d)).wait_recv()
        part = part + z1recv[d].astype(f32)
    own = e * tp + t
    seg[own] = part.astype(bf16)

    def share(slot, ssem, dev):
        start(remote(seg.at[slot], seg.at[slot], ssem, gr_sem.at[slot], dev))

    def arrived(slot):
        remote(seg.at[slot], seg.at[slot], gz_sem.at[0], gr_sem.at[slot], partner).wait_recv()

    for d in range(1, nz):
        share(own, gz_sem.at[d], z_dev(d))
    for d in range(nz):
        slot = e * tp + zpeer(d) * 2 + c
        if d:
            arrived(slot)
        for k in range(1, ep):
            share(slot, ge_sem.at[d, k], e_dev(k))
        share(slot, gp_sem.at[0, d], partner)
    for d in range(nz):
        for k in range(1, ep):
            slot = epeer(k) * tp + zpeer(d) * 2 + c
            arrived(slot)
            share(slot, gp_sem.at[k, d], partner)
    for d in range(nz):
        for k in range(ep):
            arrived(epeer(k) * tp + zpeer(d) * 2 + (1 - c))
    for d in range(1, ep):
        remote(wsend.at[d], wall.at[epeer(d)], ws_sem.at[d], wr_sem.at[ep - d], e_dev(d)).wait_recv()

    def norm_group(g, carry):
        total = jnp.zeros((rows, cols), f32)
        for b in range(tp):
            x = seg[g * tp + b].astype(f32)
            total = total + x * x
        scale = lax.rsqrt(jnp.sum(total, axis=1, keepdims=True) / width + RMS_EPS)
        spot = pl.ds(pl.multiple_of(g * rows, rows), rows)
        for b in range(tp):
            lanes = slice(b * cols, (b + 1) * cols)
            xn[spot, lanes] = (seg[g * tp + b].astype(f32) * scale * gain[:, lanes]).astype(bf16)
        return carry

    lax.fori_loop(0, ep, norm_group, 0)
    for load in loads[1:]:
        load.wait()

    total_rows = ep * rows
    step = min(total_rows, 256)

    def hidden_rows(m, carry):
        spot = pl.ds(pl.multiple_of(m * step, step), step)
        for low in range(0, ff, 256):
            high = min(ff, low + 256)
            gate = jnp.dot(xn[spot, :], wg[:, low:high], preferred_element_type=f32)
            upward = jnp.dot(xn[spot, :], wu[:, low:high], preferred_element_type=f32)
            hid[spot, low:high] = (gate / (1.0 + jnp.exp(-gate)) * upward).astype(bf16)
        return carry

    lax.fori_loop(0, total_rows // step, hidden_rows, 0)

    def down(index):
        part = jnp.dot(hid[...], block_of(wd, index), preferred_element_type=f32)
        return part.reshape(ep, rows, cols) * wall[...][:, :, :1]

    for d in far:
        p4send[d] = down(zpeer(d) * 2 + (1 - c)).astype(bf16)
        start(remote(p4send.at[d], p4recv.at[d], p4s_sem.at[d], p4r_sem.at[d], partner))
    for d in far:
        part = down(zpeer(d) * 2 + c)
        remote(p4send.at[d], p4recv.at[d], p4s_sem.at[d], p4r_sem.at[d], partner).wait_recv()
        summed[...] = part + p4recv[d].astype(f32)
        e4send[d] = summed[...].astype(bf16)
        kept[d] = summed[e]
        for k in range(1, ep):
            start(
                remote(
                    e4send.at[d, epeer(k)], e4recv.at[d, k], e4s_sem.at[d, k], e4r_sem.at[d, k], e_dev(k)
                )
            )
    for d in far:
        part = kept[d]
        for k in range(1, ep):
            remote(
                e4send.at[d, epeer(k)], e4recv.at[d, k], e4s_sem.at[d, k], e4r_sem.at[d, k], e_dev(k)
            ).wait_recv()
            part = part + e4recv[d, k].astype(f32)
        if d:
            z4send[d] = part.astype(bf16)
            start(remote(z4send.at[d], z4recv.at[d], z4s_sem.at[d], z4r_sem.at[d], z_dev(d)))
    for d in range(1, nz):
        remote(z4send.at[d], z4recv.at[d], z4s_sem.at[d], z4r_sem.at[d], z_dev(d)).wait_recv()
        part = part + z4recv[d].astype(f32)
    out[...] = (seg[own].astype(f32) + part).astype(bf16)
    for copy in started:
        copy.wait_send()


def local(
    tokens,
    state,
    routes,
    route_logits,
    mix_gain,
    w_recept,
    w_key,
    w_value,
    w_decay,
    w_rate,
    decay_base,
    rate_base,
    key_gain,
    group_gain,
    w_output,
    ffn_gain,
    w_gate,
    w_up,
    w_down,
):
    seq_rows, full_width = tokens.shape
    mixed_rows, new_state = mix_heads(
        tokens,
        state,
        mix_gain,
        (w_recept, w_key, w_value, w_decay, w_rate),
        (decay_base, rate_base, key_gain, group_gain),
    )
    ep, tp = lax.axis_size("ep"), lax.axis_size("tp")
    nz = tp // 2
    cols = full_width // tp
    ff = w_gate.shape[2]
    heads_wide = w_output.shape[0]
    f32, bf16 = jnp.float32, jnp.bfloat16
    dma = pltpu.SemaphoreType.DMA
    vmem = pl.BlockSpec(memory_space=pltpu.VMEM)
    hbm = pl.BlockSpec(memory_space=pl.ANY)
    block = (nz, seq_rows, cols)
    output = pl.pallas_call(
        experts_kernel,
        out_shape=jax.ShapeDtypeStruct((seq_rows, cols), bf16),
        in_specs=[vmem] * 5 + [hbm] * 4,
        out_specs=vmem,
        scratch_shapes=[
            pltpu.VMEM((heads_wide, full_width), bf16),
            pltpu.VMEM((full_width, ff), bf16),
            pltpu.VMEM((full_width, ff), bf16),
            pltpu.VMEM((ff, full_width), bf16),
            pltpu.VMEM(block, bf16),
            pltpu.VMEM(block, bf16),
            pltpu.VMEM(block, bf16),
            pltpu.VMEM(block, bf16),
            pltpu.VMEM((ep * tp, seq_rows, cols), bf16),
            pltpu.VMEM((ep, seq_rows, 128), f32),
            pltpu.VMEM((ep, seq_rows, 128), f32),
            pltpu.VMEM((ep * seq_rows, full_width), bf16),
            pltpu.VMEM((ep * seq_rows, ff), bf16),
            pltpu.VMEM((nz, ep, seq_rows, cols), bf16),
            pltpu.VMEM((nz, ep, seq_rows, cols), bf16),
            pltpu.VMEM((nz, ep, seq_rows, cols), bf16),
            pltpu.VMEM((nz, ep, seq_rows, cols), bf16),
            pltpu.VMEM((ep, seq_rows, cols), f32),
            pltpu.VMEM(block, f32),
            pltpu.VMEM(block, bf16),
            pltpu.VMEM(block, bf16),
            dma((4,)),
            dma((ep,)),
            dma((ep,)),
            dma((nz,)),
            dma((nz,)),
            dma((nz,)),
            dma((nz,)),
            dma((nz,)),
            dma((nz, ep)),
            dma((ep, nz)),
            dma((ep * tp,)),
            dma((nz,)),
            dma((nz,)),
            dma((nz, ep)),
            dma((nz, ep)),
            dma((nz,)),
            dma((nz,)),
        ],
        compiler_params=pltpu.CompilerParams(
            collective_id=0, has_side_effects=True, vmem_limit_bytes=67043328
        ),
    )(mixed_rows, tokens, routes.T, route_logits.T, ffn_gain[None], w_output, w_gate, w_up, w_down)
    return (output, new_state)


def solution(mesh):
    placed = (
        P("ep", None),
        P("ep", "tp", None, None),
        P("ep", None),
        P("ep", None),
        P(),
        P(None, "tp"),
        P(None, "tp"),
        P(None, "tp"),
        P(None, "tp"),
        P(None, "tp"),
        P("tp"),
        P("tp"),
        P("tp"),
        P("tp"),
        P("tp", None),
        P(),
        P("ep", None, "tp"),
        P("ep", None, "tp"),
        P("ep", "tp", None),
    )
    return jax.shard_map(
        local,
        mesh=mesh,
        in_specs=placed,
        out_specs=(P("ep", "tp"), P("ep", "tp", None, None)),
        check_vma=False,
    )
```

profile of v0, /device:TPU:0, one launch (start us, length us, event | category | flops | bytes accessed | tf_op | source)
XLA Modules:
  0.0 73.5 jit_solution(16581800149115292518)
XLA Ops:
  0.6 31.6 %shard_map.194 = (bf16[64,256]{1,0:T(8,128)(2,1)}, f32[64,4,64,64]{3,2,1,0:T(8,128)}) custom-call(bf16[64,2048]{1,0:T(8,128)(2,1)} %tokens.3, f32[1,2048]{1,0:T(1,128)} %bitcast.8, bf16[2048,256]{1,0:T(8,128)(2,1)} %w_recept.1, bf16[2048,256]{1,0:T(8,128)(2,1)} %w_key.1, bf16[2048,256]{1,0:T(8,128)(2,1)} %w_value.1, bf16[2048,256]{1,0:T(8,128)(2,1)} %w_decay.1, ...), custom_call_target="tpu_custom_call" | custom-call | tf_op jit(solution)/shard_map/pallas_call | solution.py:111
  32.2 39.8 %shard_map.195 = bf16[64,256]{1,0:T(8,128)(2,1)} custom-call(bf16[64,256]{1,0:T(8,128)(2,1)} %get-tuple-element.4.mixed, bf16[64,2048]{1,0:T(8,128)(2,1)} %tokens.3, s32[2,64]{1,0:T(2,128)} %bitcast.14, f32[2,64]{1,0:T(2,128)} %bitcast.15, f32[1,2048]{1,0:T(1,128)} %bitcast.9, bf16[256,2048]{1,0:T(8,128)(2,1)} %wo_hbm.1, bf16[1,2048,896]{2,1,0:T(8,128)(2,1)} %wg_hbm.1, ...), custom_call_target="tpu_custom_call" | custom-call | tf_op jit(solution)/shard_map/pallas_call | solution.py:403
  72.1 1.4 %copy.22 = bf16[64,256]{1,0:T(8,128)(2,1)} copy(bf16[64,256]{1,0:T(8,128)(2,1)} %shard_map.195) | data formatting | bytes 65536
where the time goes:
time: 73.7 us; the launch traced here: 73.5 us
  Pallas kernels  71.4 us (97%)
  local copies, waits for them, and re-layouts  1.38 us (2%)
    pallas_call x1, Pallas kernels, local(): pl.pallas_call(experts_kernel, out_shape=jax.ShapeDtypeStruct((seq_rows,...  39.8 us
    pallas_call x1, Pallas kernels, mix_heads(): pl.pallas_call(mix_kernel, grid=(rows // count,), out_shape=(jax.ShapeDty...  31.6 us

commit v1 on v0

--- a/solution.py
+++ b/solution.py
@@ -12,119 +12,154 @@
 UNIT_EPS = 6.4e-05
 
 
-def mix_kernel(
-    tokens,
-    gain,
-    w_recept,
-    w_key,
-    w_value,
-    w_decay,
-    w_rate,
-    decay_base,
-    rate_base,
-    key_gain,
-    group_gain,
-    state,
-    mixed,
-    new_state,
-    recept_s,
-    key_s,
-    decay_s,
-    unit_s,
-    pull_s,
-    value_t,
-    read_t,
-):
-    step = pl.program_id(0)
-    count, heads, wide, _ = state.shape
-    rows = tokens.shape[0]
+def mix_kernel(tokens, gain, w0, w1, w2, w3, w4, decay_base, rate_base, key_gain, group_gain, state, mixed, new_state,
+               wbuf, work, unit_s, pull_s, scan_s, decay_s, key_s, value_s, removed_s, old_read, wsem, in_sem, out_sem):
+    f32, bf16 = jnp.float32, jnp.bfloat16
+    rows, heads, wide, _ = work.shape
     cols = heads * wide
-    f32, bf16 = jnp.float32, jnp.bfloat16
-
-    @pl.when(step == 0)
-    def _():
-        values = tokens[...].astype(f32)
-        scale = lax.rsqrt(jnp.mean(values * values, axis=1, keepdims=True) + RMS_EPS)
-        normed = (values * scale * gain[...]).astype(bf16)
-
-        def project(weight):
-            return jnp.dot(normed, weight[...], preferred_element_type=f32).astype(bf16).astype(f32)
-
-        def split(ref, whole):
-            for h in range(heads):
-                ref[h] = whole[:, h * wide : (h + 1) * wide]
-
-        key = project(w_key)
-        split(key_s, key)
-        scaled = key * key_gain[...]
-        squares = scaled * scaled
-        rate = 1.0 / (1.0 + jnp.exp(-(project(w_rate) + rate_base[...])))
+    count = in_sem.shape[0]
+    chunk = rows // count
+    part = min(rows, 32)
+    loads = [pltpu.make_async_copy(w, wbuf.at[i], wsem.at[i]) for i, w in enumerate((w1, w4, w3, w0, w2))]
+
+    def fetch(b):
+        spot = pl.ds(b * chunk, chunk)
+        return pltpu.make_async_copy(state.at[spot], work.at[spot], in_sem.at[b])
+
+    def put(b):
+        spot = pl.ds(b * chunk, chunk)
+        return pltpu.make_async_copy(work.at[spot], new_state.at[spot], out_sem.at[b])
+
+    for load in loads:
+        load.start()
+    values = tokens[...].astype(f32)
+    scale = lax.rsqrt(jnp.mean(values * values, axis=1, keepdims=True) + RMS_EPS)
+    normed = (values * scale * gain[...]).astype(bf16)
+
+    def project(i):
+        loads[i].wait()
+        for b in range(i * count // 5, (i + 1) * count // 5):
+            fetch(b).start()
+        return jnp.dot(normed, wbuf[i], preferred_element_type=f32).astype(bf16).astype(f32)
+
+    def head(x, h):
+        return x[:, h * wide : (h + 1) * wide]
+
+    key = project(0)
+    scaled = key * key_gain[...]
+    squares = scaled * scaled
+    rate = 1.0 / (1.0 + jnp.exp(-(project(1) + rate_base[...])))
+    unit, pull = [], []
+    for h in range(heads):
+        length = jnp.sum(head(squares, h), axis=1, keepdims=True)
+        unit.append(head(scaled, h) * lax.rsqrt(length + UNIT_EPS))
+        pull.append(unit[h] * head(rate, h))
+    open_part = 1.0 / (1.0 + jnp.exp(-(project(2) + decay_base[...])))
+    decay = jnp.exp(-jnp.exp(-0.5) * open_part)
+    recept = project(3)
+    scan = decay * recept
+    met = key * recept
+    own, lost = [], []
+    for h in range(heads):
+        unit_s[h] = unit[h]
+        scan_s[h] = head(scan, h)
+        decay_s[h] = head(decay, h)
+        key_s[h] = head(key, h)
+        pull_s[h] = pull[h]
+        own.append(jnp.sum(head(met, h), axis=1, keepdims=True))
+        lost.append(jnp.sum(pull[h] * head(recept, h), axis=1, keepdims=True))
+    value = project(4)
+    value_s[...] = value
+
+    per = max(1, 128 // wide)
+    band = wide * per
+    lane = lax.broadcasted_iota(jnp.int32, (8, band), 1) // wide
+    sub = lax.broadcasted_iota(jnp.int32, (8, band), 0)
+
+    def contract(b):
+        spot = pl.ds(b * 8 if isinstance(b, int) else pl.multiple_of(b * 8, 8), 8)
+        left = jnp.concatenate([ref[h, spot, :] for ref in (unit_s, scan_s) for h in range(heads)], axis=0).astype(bf16)
+        sums = [jnp.zeros((8, band), f32)] * (2 * heads)
+        for k in range(8):
+            right = work[b * 8 + k].reshape(cols, wide).astype(bf16)
+            got = lax.dot_general(left, right, (((1,), (1,)), ((), ())), preferred_element_type=f32)
+            for g in range(2 * heads):
+                low = (g % heads) // per * band
+                sums[g] = jnp.where(sub == k, got[g * 8 : g * 8 + 8, low : low + band], sums[g])
+        for ref, base in ((removed_s, 0), (old_read, heads)):
+            for low in range(0, heads, per):
+                piece = sums[base + low]
+                for q in range(1, per):
+                    piece = jnp.where(lane == q, sums[base + low + q], piece)
+                ref[spot, low * wide : (low + per) * wide] = piece
+
+    marks = lax.broadcasted_iota(jnp.int32, (wide, 4 * part), 1) % part
+
+    def update(first, turned, right):
         for h in range(heads):
-            lanes = slice(h * wide, (h + 1) * wide)
-            length = jnp.sum(squares[:, lanes], axis=1, keepdims=True)
-            unit = scaled[:, lanes] * lax.rsqrt(length + UNIT_EPS)
-            unit_s[h] = unit
-            pull_s[h] = unit * rate[:, lanes]
-        split(recept_s, project(w_recept))
-        open_part = 1.0 / (1.0 + jnp.exp(-(project(w_decay) + decay_base[...])))
-        split(decay_s, jnp.exp(-jnp.exp(-0.5) * open_part))
-        turned = project(w_value).T
-        for b in range(rows // count):
-            value_t[b] = turned[:, b * count : (b + 1) * count]
-
-    first = step * count
-    block = value_t[step]
-    lane = lax.broadcasted_iota(jnp.int32, (wide, count), 1)
+            left = turned[h * wide : (h + 1) * wide, :]
+            stack = jnp.concatenate(
+                [jnp.where(marks == (first + k) % part, left, 0.0).astype(bf16) for k in range(8)], axis=0
+            )
+            delta = jnp.dot(stack, right[h], preferred_element_type=f32)
+            for k in range(8):
+                s = first + k
+                work[s, h] = work[s, h] * decay_s[h, s : s + 1, :] + delta[k * wide : (k + 1) * wide]
+
+    per_chunk = chunk // 8
+    for g in range(rows // part):
+        span = slice(g * part, (g + 1) * part)
+        for b in range(g * part // 8, (g + 1) * part // 8):
+            if b % per_chunk == 0:
+                fetch(b // per_chunk).wait()
+            contract(b)
+        removed = removed_s[span, :]
+        high = removed.astype(bf16).astype(f32)
+        turned = jnp.concatenate([high, removed - high, value_s[span, :], high], axis=0).T
+        right = []
+        for h in range(heads):
+            p = pull_s[h, span, :]
+            hi = p.astype(bf16).astype(f32)
+            right.append(jnp.concatenate([-hi, -hi, key_s[h, span, :], hi - p], axis=0).astype(bf16))
+        for b in range(g * part // 8, (g + 1) * part // 8):
+            update(b * 8, turned, right)
+            if (b + 1) % per_chunk == 0:
+                put(b // per_chunk).start()
+    removed = removed_s[...]
+    old = old_read[...]
     for h in range(heads):
-        read = jnp.zeros((wide, count), f32)
-        for k in range(count):
-            spot = pl.ds(first + k, 1)
-            old = state[k, h]
-            removed = jnp.sum(old * unit_s[h, spot, :], axis=1, keepdims=True)
-            column = block[h * wide : (h + 1) * wide, k : k + 1]
-            new = old * decay_s[h, spot, :] - removed * pull_s[h, spot, :] + column * key_s[h, spot, :]
-            new_state[k, h] = new
-            out = jnp.sum(new * recept_s[h, spot, :], axis=1, keepdims=True)
-            read = jnp.where(lane == k, out, read)
-        centred = read - jnp.mean(read, axis=0, keepdims=True)
-        spread = jnp.mean(centred * centred, axis=0, keepdims=True)
-        read_t[step, h * wide : (h + 1) * wide, :] = centred * lax.rsqrt(spread + GROUP_EPS)
-
-    @pl.when(step == rows // count - 1)
-    def _():
-        whole = jnp.concatenate([read_t[b] for b in range(rows // count)], axis=1)
-        mixed[...] = (whole.T * group_gain[...]).astype(bf16)
+        lanes = slice(h * wide, (h + 1) * wide)
+        out = old[:, lanes] - removed[:, lanes] * lost[h] + value[:, lanes] * own[h]
+        centred = out - jnp.mean(out, axis=1, keepdims=True)
+        spread = jnp.mean(centred * centred, axis=1, keepdims=True)
+        mixed[:, lanes] = (centred * lax.rsqrt(spread + GROUP_EPS) * group_gain[:, lanes]).astype(bf16)
+    for b in range(count):
+        put(b).wait()
 
 
 def mix_heads(tokens, state, mix_gain, projections, offsets):
     rows, width = tokens.shape
     _, heads, wide, _ = state.shape
     cols = heads * wide
-    count = min(rows, 8)
+    count = rows // 8
     f32 = jnp.float32
-
-    def whole(*shape):
-        return pl.BlockSpec(shape, lambda i: (0,) * len(shape))
-
-    states = pl.BlockSpec((count, heads, wide, wide), lambda i: (i, 0, 0, 0))
+    vmem = pl.BlockSpec(memory_space=pltpu.VMEM)
+    hbm = pl.BlockSpec(memory_space=pl.ANY)
     per_head = pltpu.VMEM((heads, rows, wide), f32)
+    flat = pltpu.VMEM((rows, cols), f32)
     return pl.pallas_call(
         mix_kernel,
-        grid=(rows // count,),
         out_shape=(
             jax.ShapeDtypeStruct((rows, cols), jnp.bfloat16),
             jax.ShapeDtypeStruct(state.shape, f32),
         ),
-        in_specs=[whole(rows, width), whole(1, width)]
-        + [whole(width, cols)] * 5
-        + [whole(1, cols)] * 4
-        + [states],
-        out_specs=(whole(rows, cols), states),
-        scratch_shapes=[per_head] * 5
-        + [pltpu.VMEM((rows // count, cols, count), f32)] * 2,
-        compiler_params=pltpu.CompilerParams(
-            dimension_semantics=("arbitrary",), vmem_limit_bytes=67043328
-        ),
+        in_specs=[vmem] * 2 + [hbm] * 5 + [vmem] * 4 + [hbm],
+        out_specs=(vmem, hbm),
+        scratch_shapes=[pltpu.VMEM((5, width, cols), jnp.bfloat16), pltpu.VMEM(state.shape, f32)]
+        + [per_head] * 5
+        + [flat] * 3
+        + [pltpu.SemaphoreType.DMA((5,)), pltpu.SemaphoreType.DMA((count,)), pltpu.SemaphoreType.DMA((count,))],
+        compiler_params=pltpu.CompilerParams(vmem_limit_bytes=67043328),
     )(tokens, mix_gain[None], *projections, *[x[None] for x in offsets], state)
 
 

time: 73.7 us -> 53.2 us (0.72)
  Pallas kernels: 71.4 us -> 51 us
    pallas_call x1, Pallas kernels: 31.6 us -> 11.1 us  [mix_heads(): pl.pallas_call(mix_kernel, out_shape=(jax.ShapeDtypeStruct((rows, cols),...]
where the time goes in v1:
time: 53.2 us; the launch traced here: 53 us
  Pallas kernels  51 us (96%)
  local copies, waits for them, and re-layouts  1.38 us (3%)
  between operations  0.65 us (1%)
    pallas_call x1, Pallas kernels, local(): pl.pallas_call(experts_kernel, out_shape=jax.ShapeDtypeStruct((seq_rows,...  39.9 us
    pallas_call x1, Pallas kernels, mix_heads(): pl.pallas_call(mix_kernel, out_shape=(jax.ShapeDtypeStruct((rows, cols),...  11.1 us
    unnamed x1, local copies, waits for them, and re-layouts  1.38 us

profile of v1, /device:TPU:0, one launch (start us, length us, event | category | flops | bytes accessed | tf_op | source)
XLA Modules:
  0.0 53.0 jit_solution(4391809626787586844)
XLA Ops:
  0.6 11.1 %shard_map.194 = (bf16[64,256]{1,0:T(8,128)(2,1)}, f32[64,4,64,64]{3,2,1,0:T(8,128)}) custom-call(bf16[64,2048]{1,0:T(8,128)(2,1)} %tokens.3, f32[1,2048]{1,0:T(1,128)} %bitcast.8, bf16[2048,256]{1,0:T(8,128)(2,1)} %w0.1, bf16[2048,256]{1,0:T(8,128)(2,1)} %w1.1, bf16[2048,256]{1,0:T(8,128)(2,1)} %w2.1, bf16[2048,256]{1,0:T(8,128)(2,1)} %w3.1, ...), custom_call_target="tpu_custom_call" | custom-call | tf_op jit(solution)/shard_map/pallas_call | solution.py:150
  11.8 39.9 %shard_map.195 = bf16[64,256]{1,0:T(8,128)(2,1)} custom-call(bf16[64,256]{1,0:T(8,128)(2,1)} %get-tuple-element.4.mixed, bf16[64,2048]{1,0:T(8,128)(2,1)} %tokens.3, s32[2,64]{1,0:T(2,128)} %bitcast.14, f32[2,64]{1,0:T(2,128)} %bitcast.15, f32[1,2048]{1,0:T(1,128)} %bitcast.9, bf16[256,2048]{1,0:T(8,128)(2,1)} %wo_hbm.1, bf16[1,2048,896]{2,1,0:T(8,128)(2,1)} %wg_hbm.1, ...), custom_call_target="tpu_custom_call" | custom-call | tf_op jit(solution)/shard_map/pallas_call | solution.py:438
  51.6 1.4 %copy.22 = bf16[64,256]{1,0:T(8,128)(2,1)} copy(bf16[64,256]{1,0:T(8,128)(2,1)} %shard_map.195) | data formatting | bytes 65536
